TPU v7x, 32 devices: a whole 2x2x4 slice. The times are simulated.
32 devices in a mesh: ep: 8 (over z, y), tp: 4 (over x, core).
Axes of the slice: x: 2, y: 2, z: 4, core: 2. Of those that a mesh axis runs over, the one named last changes fastest.
Arguments:
- hidden: bfloat16 [256, 2048], P('ep')
- norm_gains: float32 [4, 2048], replicated, may hold values from 0.1 to 1.9
- w_query: bfloat16 [2048, 1024], P(None, 'tp'), may hold values from -0.125 to 0.125
- w_key: bfloat16 [2048, 1024], P(None, 'tp'), may hold values from -0.125 to 0.125
- w_value: bfloat16 [2048, 1024], P(None, 'tp'), may hold values from -0.125 to 0.125
- w_outgate: bfloat16 [2048, 1024], P(None, 'tp'), may hold values from -0.125 to 0.125
- w_input_gate: bfloat16 [2048, 8], replicated, may hold values from -0.125 to 0.125
- w_forget_gate: bfloat16 [2048, 8], replicated, may hold values from -0.125 to 0.125
- forget_bias: float32 [8], replicated, may hold values from -1 to 4
- w_mix_out: bfloat16 [1024, 2048], P('tp')
- state_matrix: float32 [256, 8, 128, 128], P('ep', 'tp'), may hold values from -0.6 to 0.6
- state_norm: float32 [256, 8, 128], P('ep', 'tp'), may hold values from -0.6 to 0.6
- state_max: float32 [256, 8], P('ep', 'tp'), may hold values from -4 to 4
- routes: int32 [256, 2], P('ep'), may hold values from 0 to 7, all different within a row; in each aligned block of 32 rows (0 to 31, 32 to 63, ...) at most 16 rows name the same one
- route_scores: float32 [256, 2], P('ep'), may hold values from 0.1 to 1
- expert_gate: bfloat16 [8, 2048, 3584], P('ep', None, 'tp'), may hold values from -0.125 to 0.125
- expert_up: bfloat16 [8, 2048, 3584], P('ep', None, 'tp'), may hold values from -0.125 to 0.125
- expert_down: bfloat16 [8, 3584, 2048], P('ep', 'tp')
- dense_gate: bfloat16 [2048, 5632], P('tp', 'ep'), may hold values from -0.125 to 0.125
- dense_up: bfloat16 [2048, 5632], P('tp', 'ep'), may hold values from -0.125 to 0.125
- dense_down: bfloat16 [5632, 2048], P('ep', 'tp')
- dense_mix: float32 [2048], replicated, may hold values from -0.25 to 0.25
Outputs:
- new_hidden: bfloat16 [256, 2048], P('ep', 'tp')
- new_matrix: float32 [256, 8, 128, 128], P('ep', 'tp')
- new_norm: float32 [256, 8, 128], P('ep', 'tp')
- new_max: float32 [256, 8], P('ep', 'tp')
Inputs may be any that keep to these rules, and one draw needn't show every extreme that they name: `routes`: each row names 2 different experts. Among the rows of one index of ep (an aligned block of 32 rows) no expert is named by more than 16 rows, and in every draw some expert is named by exactly 16 rows of some block.
All inputs are finite; a program needn't handle non-finite values.
Results may differ from a plain program's by a relative error of at most 0.02.
Values may be sent and summed in bfloat16 or wider, within the bound.
No kernel may reach another device: no remote copies, remote signals or barrier semaphores. Data moves between devices by JAX's collectives and lax.ppermute only.
A program may use at most 128 MiB of HBM per device.

v0:
```python
import jax
import jax.numpy as jnp
from jax import lax
from jax.sharding import PartitionSpec as P

EPS = 1e-06


def settle(values):
    return lax.optimization_barrier(values.astype(jnp.bfloat16)).astype(jnp.float32)


def local(
    hidden,
    norm_gains,
    w_query,
    w_key,
    w_value,
    w_outgate,
    w_input_gate,
    w_forget_gate,
    forget_bias,
    w_mix_out,
    state_matrix,
    state_norm,
    state_max,
    routes,
    route_scores,
    expert_gate,
    expert_up,
    expert_down,
    dense_gate,
    dense_up,
    dense_down,
    dense_mix,
):
    tp_count = lax.axis_size("tp")
    ep_count = lax.axis_size("ep")
    tp_place = lax.axis_index("tp")
    seq_local, width = hidden.shape
    heads_local = state_matrix.shape[1]
    head_width = state_matrix.shape[2]
    part_width = width // tp_count
    feature_first = tp_place * part_width
    start_f = hidden.astype(jnp.float32)
    normed_in = (
        start_f
        * lax.rsqrt(jnp.mean(start_f * start_f, axis=-1, keepdims=True) + EPS)
        * norm_gains[0]
    ).astype(jnp.bfloat16)
    query_f = jnp.dot(normed_in, w_query, preferred_element_type=jnp.float32)
    key_f = jnp.dot(normed_in, w_key, preferred_element_type=jnp.float32)
    value_f = jnp.dot(normed_in, w_value, preferred_element_type=jnp.float32)
    gate_f = jnp.dot(normed_in, w_outgate, preferred_element_type=jnp.float32)
    head_first = tp_place * heads_local
    input_weight = lax.dynamic_slice_in_dim(w_input_gate, head_first, heads_local, 1)
    forget_weight = lax.dynamic_slice_in_dim(w_forget_gate, head_first, heads_local, 1)
    forget_local = lax.dynamic_slice_in_dim(forget_bias, head_first, heads_local, 0)
    in_gate = jnp.dot(normed_in, input_weight, preferred_element_type=jnp.float32)
    log_forget = jax.nn.log_sigmoid(
        jnp.dot(normed_in, forget_weight, preferred_element_type=jnp.float32) + forget_local
    )
    query = settle(query_f).reshape(seq_local, heads_local, head_width)
    keys = settle(key_f).reshape(seq_local, heads_local, head_width) * head_width ** (-0.5)
    values = settle(value_f).reshape(seq_local, heads_local, head_width)
    carried = log_forget + state_max
    new_max = jnp.maximum(carried, in_gate)
    keep = jnp.exp(carried - new_max)
    write = jnp.exp(in_gate - new_max)
    written = write[:, :, None] * keys
    new_matrix = (
        keep[:, :, None, None] * state_matrix + written[:, :, :, None] * values[:, :, None, :]
    )
    new_norm = keep[:, :, None] * state_norm + written
    numer = jnp.einsum("shd,shdv->shv", query, new_matrix)
    denom = jnp.einsum("shd,shd->sh", query, new_norm)
    read = numer / jnp.maximum(jnp.abs(denom), jnp.exp(-new_max))[:, :, None]
    mixed = (
        jax.nn.sigmoid(settle(gate_f)) * read.reshape(seq_local, heads_local * head_width)
    ).astype(jnp.bfloat16)
    branch_terms = settle(jnp.dot(mixed, w_mix_out, preferred_element_type=jnp.float32))
    branch = settle(
        lax.psum_scatter(
            branch_terms.astype(jnp.bfloat16), "tp", scatter_dimension=1, tiled=True
        ).astype(jnp.float32)
    )
    start_part = lax.dynamic_slice_in_dim(start_f, feature_first, part_width, 1)
    gain_rows = lax.dynamic_slice_in_dim(norm_gains, feature_first, part_width, 1)
    lifted = gain_rows[1] * branch
    mix_weight = gain_rows[2] * lax.dynamic_slice_in_dim(dense_mix, feature_first, part_width, 0)
    branch_sq, start_sq, cross_sum, lifted_sq, start_dot, lifted_dot = lax.psum(
        (
            jnp.sum(branch * branch, axis=-1),
            jnp.sum(start_part * start_part, axis=-1),
            jnp.sum(start_part * lifted, axis=-1),
            jnp.sum(lifted * lifted, axis=-1),
            jnp.sum(start_part * mix_weight, axis=-1),
            jnp.sum(lifted * mix_weight, axis=-1),
        ),
        "tp",
    )
    branch_scale = lax.rsqrt(branch_sq / width + EPS)
    residual_f = start_part + lifted * branch_scale[:, None]
    resid_sq = start_sq + 2.0 * branch_scale * cross_sum + branch_scale * branch_scale * lifted_sq
    gate_dot = start_dot + branch_scale * lifted_dot
    scale_two = lax.rsqrt(resid_sq / width + EPS)
    mix_gate = jax.nn.sigmoid(scale_two * gate_dot)
    residual = settle(residual_f)
    normed = (residual_f * scale_two[:, None] * gain_rows[2]).astype(jnp.bfloat16)
    rows_in = lax.all_gather(normed, "ep", axis=0, tiled=True)
    dense_pre = jnp.concatenate(
        [
            jnp.dot(rows_in, dense_gate, preferred_element_type=jnp.float32),
            jnp.dot(rows_in, dense_up, preferred_element_type=jnp.float32),
        ],
        axis=1,
    )
    dense_pre = lax.psum(dense_pre.astype(jnp.bfloat16), "tp").astype(jnp.float32)
    dense_pre_gate, dense_pre_up = jnp.split(dense_pre, 2, axis=1)
    dense_hidden = (jax.nn.silu(dense_pre_gate) * dense_pre_up).astype(jnp.bfloat16)
    dense_out = lax.psum_scatter(
        jnp.dot(dense_hidden, dense_down, preferred_element_type=jnp.float32).astype(jnp.bfloat16),
        "ep",
        scatter_dimension=0,
        tiled=True,
    ).astype(jnp.float32)
    route_width = routes.shape[1]
    expert_count = ep_count * expert_gate.shape[0]
    capacity = 2 * seq_local * route_width // ep_count
    flat_expert = routes.reshape(-1)
    picks = (flat_expert[:, None] == jnp.arange(expert_count, dtype=jnp.int32)[None, :]).astype(
        jnp.int32
    )
    ranks = jnp.sum(jnp.cumsum(picks, axis=0) * picks, axis=1) - 1
    slot_index = flat_expert * capacity + ranks
    placing = (
        jnp.arange(expert_count * capacity, dtype=jnp.int32)[:, None] == slot_index[None, :]
    ).astype(jnp.bfloat16)
    repeated = jnp.repeat(normed, route_width, axis=0)
    outgoing = (
        jnp.dot(placing, repeated, preferred_element_type=jnp.float32)
        .astype(jnp.bfloat16)
        .reshape(expert_count, capacity, part_width)
    )
    arrived = lax.all_to_all(outgoing, "ep", split_axis=0, concat_axis=0, tiled=True)
    full_rows = lax.all_gather(arrived, "tp", axis=2, tiled=True)
    flat_rows = full_rows.reshape(-1, width)
    gate_pre = jnp.dot(flat_rows, expert_gate[0], preferred_element_type=jnp.float32)
    up_pre = jnp.dot(flat_rows, expert_up[0], preferred_element_type=jnp.float32)
    hidden_units = (jax.nn.silu(gate_pre) * up_pre).astype(jnp.bfloat16)
    partial_out = settle(jnp.dot(hidden_units, expert_down[0], preferred_element_type=jnp.float32))
    summed_out = lax.psum_scatter(
        partial_out.astype(jnp.bfloat16), "tp", scatter_dimension=1, tiled=True
    )
    returned = lax.all_to_all(
        summed_out.reshape(arrived.shape), "ep", split_axis=0, concat_axis=0, tiled=True
    )
    picked = lax.dot_general(
        placing,
        returned.reshape(expert_count * capacity, part_width),
        (((0,), (0,)), ((), ())),
        preferred_element_type=jnp.float32,
    )
    share = route_scores / jnp.sum(route_scores, axis=-1, keepdims=True)
    moe_out = jnp.sum(
        picked.reshape(seq_local, route_width, part_width) * share[:, :, None], axis=1
    )
    ffn = moe_out + mix_gate[:, None] * dense_out
    ffn_sq = lax.psum(jnp.sum(ffn * ffn, axis=-1), "tp")
    new_hidden = (residual + gain_rows[3] * ffn * lax.rsqrt(ffn_sq / width + EPS)[:, None]).astype(
        jnp.bfloat16
    )
    return (new_hidden, new_matrix, new_norm, new_max)


def solution(mesh):
    placed = (
        P("ep", None),
        P(),
        P(None, "tp"),
        P(None, "tp"),
        P(None, "tp"),
        P(None, "tp"),
        P(),
        P(),
        P(),
        P("tp", None),
        P("ep", "tp", None, None),
        P("ep", "tp", None),
        P("ep", "tp"),
        P("ep", None),
        P("ep", None),
        P("ep", None, "tp"),
        P("ep", None, "tp"),
        P("ep", "tp", None),
        P("tp", "ep"),
        P("tp", "ep"),
        P("ep", "tp"),
        P(),
    )
    return jax.shard_map(
        local,
        mesh=mesh,
        in_specs=placed,
        out_specs=(P("ep", "tp"), P("ep", "tp", None, None), P("ep", "tp", None), P("ep", "tp")),
        check_vma=False,
    )
```

profile of v0, /device:TPU:0, one launch (start us, length us, event | category | flops | bytes accessed | tf_op | source)
XLA Modules:
  0.0 237.0 jit_solution(14512095781934341025)
XLA Ops:
  7.2 0.0 copy-start
  7.2 0.0 copy-start.2
  7.2 0.0 reduce-scatter.4.cloned.1.call-start
  7.3 0.9 slice.14
  8.2 1.0 multiply_reduce_fusion
  9.2 1.6 convolution_convert_fusion.7
  10.9 1.1 fusion.44
  12.0 0.7 dynamic_slice.21
  12.8 1.2 subtract_exponential_fusion
  13.9 0.0 copy-start.7
  14.0 0.1 copy.32
  14.0 0.1 copy.31
  14.1 1.6 convolution_convert_fusion.6
  15.8 1.6 convolution_convert_fusion.5
  17.5 0.8 fusion.38
  18.2 0.1 copy.42
  18.3 0.1 copy.34
  18.4 0.3 convolution_convert_fusion.8
  18.7 3.7 %multiply_add_fusion = f32[32,2,128,128]{3,2,1,0:T(8,128)S(1)} fusion(f32[32,2,128,128]{3,2,1,0:T(8,128)} %param.32, f32[32,2,128]{2,1,0:T(2,128)S(1)} %reshape.112, f32[32,2,128]{2,1,0:T(2,128)S(1)} %get-tuple-element.20, f32[32,2]{1,0:T(8,128)S(1)} %copy.31), kind=kLoop, calls=%fused_computation | loop fusion | flops 3145728 | bytes 8454400 | tf_op jit(solution)/shard_map/add | solution.py:72
  22.4 0.0 copy-start.1
  22.5 2.0 copy-done.1
  24.5 0.6 fusion.57
  25.1 0.1 broadcast_divide_fusion
  25.3 0.9 convolution_convert_fusion
  26.2 0.0 reduce-scatter.4.cloned.1.call-update
  26.2 0.1 copy.35
  26.3 0.1 reshape.104
  26.4 0.1 fusion.40
  26.5 0.1 reduce_window_sum.11
  26.6 0.2 select_reduce_fusion
  26.8 0.9 fusion.56
  27.7 0.8 dynamic-slice_multiply_fusion
  28.5 20.2 %reduce-scatter.4.cloned.1.call-done = bf16[32,512]{1,0:T(8,128)(2,1)} async-done(((bf16[32,2048]{1,0:T(8,128)(2,1)}), bf16[32,512]{1,0:T(8,128)(2,1)}) %reduce-scatter.4.cloned.1.call-update) | async-done | bytes 32784 | tf_op jit(solution)/shard_map/reduce_scatter | solution.py:83
  48.7 1.0 multiply_reduce_fusion.2
  49.7 5.8 %all-reduce = (f32[32]{0:T(128)S(1)}, f32[32]{0:T(128)S(1)}, f32[32]{0:T(128)S(1)}, f32[32]{0:T(128)S(1)}, f32[32]{0:T(128)S(1)}, /*index=5*/f32[32]{0:T(128)S(1)}) all-reduce(f32[32]{0:T(128)S(1)} %get-tuple-element.9, f32[32]{0:T(128)S(1)} %get-tuple-element.8, f32[32]{0:T(128)S(1)} %get-tuple-element.5, ...), channel_id=1, replica_groups=mesh['ep'=8,'tp'=4] {'tp'}, use_global_device_ids=true, to_apply=%region_3.4 | all-reduce | flops 192 | bytes 1536 | tf_op jit(solution)/shard_map/psum | solution.py:91
  55.5 0.9 multiply_convert_fusion.1
  56.3 31.2 %all_gather.7 = bf16[256,512]{1,0:T(8,128)(2,1)S(1)} all-gather(bf16[32,512]{1,0:T(8,128)(2,1)S(1)} %get-tuple-element.23), channel_id=1, replica_groups=mesh['ep'=8,'tp'=4] {'ep'}, dimensions={0}, use_global_device_ids=true | all-gather | bytes 294912 | tf_op jit(solution)/shard_map/all_gather | solution.py:110
  87.5 0.4 convolution_convert_fusion.1
  87.9 0.4 convolution_convert_fusion.2
  88.4 0.8 convolution_convert_fusion.4
  89.2 5.3 %all-to-all-start = ((bf16[8,16,512]{2,1,0:T(8,128)(2,1)}), bf16[8,16,512]{2,1,0:T(8,128)(2,1)S(1)}, u32[]{:S(2)}, u32[]{:S(2)}) async-start(bf16[8,16,512]{2,1,0:T(8,128)(2,1)} %bitcast.6), calls=%async_computation.1 | async-start | bytes 262144 | tf_op jit(solution)/shard_map/all_to_all | solution.py:145
  94.5 0.0 all-reduce.3.cloned.1.call-start
  94.5 0.9 pad_maximum_fusion
  95.4 0.0 all-reduce.3.cloned.1.call-update
  95.5 0.0 reduce-scatter.6.cloned.1.call-start
  95.5 6.3 %all-to-all-done = bf16[8,16,512]{2,1,0:T(8,128)(2,1)S(1)} async-done(((bf16[8,16,512]{2,1,0:T(8,128)(2,1)}), bf16[8,16,512]{2,1,0:T(8,128)(2,1)S(1)}, u32[]{:S(2)}, u32[]{:S(2)}) %all-to-all-start) | async-done | bytes 131104 | tf_op jit(solution)/shard_map/all_to_all | solution.py:145
  101.8 9.2 %all_gather.6 = bf16[8,16,2048]{2,1,0:T(8,128)(2,1)S(1)} all-gather(bf16[8,16,512]{2,1,0:T(8,128)(2,1)S(1)} %all-to-all-done), channel_id=1, replica_groups=mesh['ep'=8,'tp'=4] {'tp'}, dimensions={2}, use_global_device_ids=true | all-gather | bytes 655360 | tf_op jit(solution)/shard_map/all_gather | solution.py:146
  111.0 2.8 %fusion.4 = f32[128,896]{1,0:T(8,128)S(1)} fusion(bf16[128,2048]{1,0:T(8,128)(2,1)S(1)} %bitcast.51, bf16[1,2048,896]{2,1,0:T(8,128)(2,1)} %param.37), kind=kOutput, calls=%fused_computation.5 | convolution fusion | flops 469762048 | bytes 4653056 | tf_op jit(solution)/shard_map/dot_general | solution.py:148
  113.9 5.5 %fusion.6 = bf16[128,2048]{1,0:T(8,128)(2,1)} fusion(bf16[1,896,2048]{2,1,0:T(8,128)(2,1)} %param.39, bf16[128,2048]{1,0:T(8,128)(2,1)S(1)} %bitcast.52, bf16[1,2048,896]{2,1,0:T(8,128)(2,1)} %param.38, f32[128,896]{1,0:T(8,128)S(1)} %fusion.4), kind=kOutput, calls=%fused_computation.7 | convolution fusion | flops 940474368 | bytes 8847360 | tf_op jit(solution)/shard_map/dot_general | solution.py:151
  119.3 0.0 reduce-scatter.6.cloned.1.call-update
  119.3 0.0 reduce-scatter.8.cloned.1.call-start
  119.4 13.2 %all-reduce.3.cloned.1.call-done = bf16[256,1408]{0,1:T(8,128)(2,1)} async-done(((bf16[256,1408]{0,1:T(8,128)(2,1)}), bf16[256,1408]{0,1:T(8,128)(2,1)}) %all-reduce.3.cloned.1.call-update) | async-done | bytes 720912 | tf_op jit(solution)/shard_map/psum | solution.py:118
  132.6 1.2 convert_element_type.94
  133.8 1.1 convolution_convert_fusion.3
  134.9 0.0 reduce-scatter.8.cloned.1.call-update
  134.9 21.8 %reduce-scatter.6.cloned.1.call-done = bf16[128,512]{1,0:T(8,128)(2,1)} async-done(((bf16[128,2048]{1,0:T(8,128)(2,1)}), bf16[128,512]{1,0:T(8,128)(2,1)}) %reduce-scatter.6.cloned.1.call-update) | async-done | bytes 131088 | tf_op jit(solution)/shard_map/reduce_scatter | solution.py:152
  156.7 5.5 %all-to-all-start.1 = ((bf16[8,16,512]{2,1,0:T(8,128)(2,1)}), bf16[8,16,512]{2,1,0:T(8,128)(2,1)S(1)}, u32[]{:S(2)}, u32[]{:S(2)}) async-start(bf16[8,16,512]{2,1,0:T(8,128)(2,1)} %bitcast.62), calls=%async_computation.3 | async-start | bytes 262144 | tf_op jit(solution)/shard_map/all_to_all | solution.py:155
  162.3 0.1 iota_compare_fusion.3
  162.4 7.2 %all-to-all-done.1 = bf16[8,16,512]{2,1,0:T(8,128)(2,1)S(1)} async-done(((bf16[8,16,512]{2,1,0:T(8,128)(2,1)}), bf16[8,16,512]{2,1,0:T(8,128)(2,1)S(1)}, u32[]{:S(2)}, u32[]{:S(2)}) %all-to-all-start.1) | async-done | bytes 131104 | tf_op jit(solution)/shard_map/all_to_all | solution.py:155
  169.6 0.2 fusion.15
  169.8 52.6 %reduce-scatter.8.cloned.1.call-done = bf16[32,512]{1,0:T(8,128)(2,1)} async-done(((bf16[256,512]{1,0:T(8,128)(2,1)}), bf16[32,512]{1,0:T(8,128)(2,1)}) %reduce-scatter.8.cloned.1.call-update) | async-done | bytes 32784 | tf_op jit(solution)/shard_map/reduce_scatter | solution.py:121
  222.4 0.9 multiply_reduce_fusion.1
  223.3 5.7 %psum.63 = f32[32]{0:T(128)S(1)} all-reduce(f32[32]{0:T(128)S(1)} %multiply_reduce_fusion.1), channel_id=1, replica_groups=mesh['ep'=8,'tp'=4] {'tp'}, use_global_device_ids=true, to_apply=%region_22.23 | all-reduce | flops 32 | bytes 256 | tf_op jit(solution)/shard_map/psum | solution.py:169
  229.0 1.5 add_convert_fusion
  (33 shorter events, 0.3 us)
Async XLA Ops:
  7.2 18.1 %copy-start = (bf16[256,2048]{1,0:T(8,128)(2,1)S(1)}, bf16[256,2048]{1,0:T(8,128)(2,1)}, u32[]{:S(2)}) copy-start(bf16[256,2048]{1,0:T(8,128)(2,1)} %param.31) | copy-start | bytes 3145732
  7.2 11.2 %copy-start.2 = (bf16[32,2048]{1,0:T(8,128)(2,1)S(1)}, bf16[32,2048]{1,0:T(8,128)(2,1)}, u32[]{:S(2)}) copy-start(bf16[32,2048]{1,0:T(8,128)(2,1)} %param.22) | copy-start | bytes 393220
  7.2 10.3 %copy-start.6 = (f32[32,2,128]{2,1,0:T(2,128)S(1)}, f32[32,2,128]{2,1,0:T(2,128)}, u32[]{:S(2)}) copy-start(f32[32,2,128]{2,1,0:T(2,128)} %param.33) | copy-start | bytes 98308
  7.2 11.2 %copy-start.3 = (bf16[2048,256]{1,0:T(8,128)(2,1)S(1)}, bf16[2048,256]{1,0:T(8,128)(2,1)}, u32[]{:S(2)}) copy-start(bf16[2048,256]{1,0:T(8,128)(2,1)} %param.27) | copy-start | bytes 3145732
  7.2 41.5 %reduce-scatter.4.cloned.1.call-start = ((), (), s32[]{:S(2)}) async-start(), calls=%async_computation.5 | async-start | bytes 163840 | tf_op jit(solution)/shard_map/reduce_scatter | solution.py:83
  13.9 8.5 %copy-start.7 = (f32[32,2]{0,1:T(2,128)}, f32[32,2]{0,1:T(2,128)S(1)}, u32[]{:S(2)}) copy-start(f32[32,2]{0,1:T(2,128)S(1)} %get-tuple-element.22) | copy-start | bytes 772
  22.4 2.0 copy-start.1
  24.5 1.7 copy-start.9
  24.5 63.0 %copy-start.4 = (bf16[512,704]{0,1:T(8,128)(2,1)S(1)}, bf16[512,704]{0,1:T(8,128)(2,1)}, u32[]{:S(2)}) copy-start(bf16[512,704]{0,1:T(8,128)(2,1)} %param.41) | copy-start | bytes 2162692
  24.5 63.4 %copy-start.5 = (bf16[512,704]{0,1:T(8,128)(2,1)S(1)}, bf16[512,704]{0,1:T(8,128)(2,1)}, u32[]{:S(2)}) copy-start(bf16[512,704]{0,1:T(8,128)(2,1)} %param.40) | copy-start | bytes 2162692
  89.2 12.6 %all-to-all-start = ((bf16[8,16,512]{2,1,0:T(8,128)(2,1)}), bf16[8,16,512]{2,1,0:T(8,128)(2,1)S(1)}, u32[]{:S(2)}, u32[]{:S(2)}) async-start(bf16[8,16,512]{2,1,0:T(8,128)(2,1)} %bitcast.6), calls=%async_computation.1 | async-start | bytes 262144 | tf_op jit(solution)/shard_map/all_to_all | solution.py:145
  94.5 38.1 %all-reduce.3.cloned.1.call-start = ((), (), s32[]{:S(2)}) async-start(), calls=%async_computation.7 | async-start | bytes 1441792 | tf_op jit(solution)/shard_map/psum | solution.py:118
  95.5 61.3 %reduce-scatter.6.cloned.1.call-start = ((), (), s32[]{:S(2)}) async-start(), calls=%async_computation.6 | async-start | bytes 655360 | tf_op jit(solution)/shard_map/reduce_scatter | solution.py:152
  113.8 19.9 %copy-start.10 = (bf16[704,512]{1,0:T(8,128)(2,1)S(1)}, bf16[704,512]{1,0:T(8,128)(2,1)}, u32[]{:S(2)}) copy-start(bf16[704,512]{1,0:T(8,128)(2,1)} %param.42) | copy-start | bytes 2162692
  119.3 43.0 %copy-start.8 = (f32[32,2]{0,1:T(2,128)S(1)}, f32[32,2]{0,1:T(2,128)}, u32[]{:S(2)}) copy-start(f32[32,2]{0,1:T(2,128)} %param.36) | copy-start | bytes 772
  119.3 103.0 %reduce-scatter.8.cloned.1.call-start = ((), (), s32[]{:S(2)}) async-start(), calls=%async_computation.8 | async-start | bytes 294912 | tf_op jit(solution)/shard_map/reduce_scatter | solution.py:121
  156.7 12.9 %all-to-all-start.1 = ((bf16[8,16,512]{2,1,0:T(8,128)(2,1)}), bf16[8,16,512]{2,1,0:T(8,128)(2,1)S(1)}, u32[]{:S(2)}, u32[]{:S(2)}) async-start(bf16[8,16,512]{2,1,0:T(8,128)(2,1)} %bitcast.62), calls=%async_computation.3 | async-start | bytes 262144 | tf_op jit(solution)/shard_map/all_to_all | solution.py:155
Sparse Core Ops, SparseCore 0:
  26.3 22.3 reduce-scatter.3
  97.7 34.8 all-reduce.2
  135.0 21.6 reduce-scatter.5
  159.9 62.4 reduce-scatter.7
where the time goes:
time: 238 us; the launch traced here: 237 us
  waiting for transfers between devices  121 us (51%)
  blocking collectives  51.8 us (22%)
  matrix products  20.2 us (8%)
  between operations  14.1 us (6%)
  other arithmetic  13.3 us (6%)
  starting transfers between devices  11 us (5%)
  local copies, waits for them, and re-layouts  5.31 us (2%)
    reduce_scatter x1, waiting for transfers between devices, local(): lax.psum_scatter(jnp.dot(dense_hidden, dense_down, preferred_element_type...  52.6 us
    all_gather x1, blocking collectives, local(): rows_in = lax.all_gather(normed, 'ep', axis=0, tiled=True)  31.2 us
    reduce_scatter x1, waiting for transfers between devices, local(): lax.psum_scatter(partial_out.astype(jnp.bfloat16), 'tp', scatter_dimensio...  21.8 us
    reduce_scatter x1, waiting for transfers between devices, local(): lax.psum_scatter(branch_terms.astype(jnp.bfloat16), 'tp', scatter_dimensi...  20.2 us
    psum x1, waiting for transfers between devices, local(): lax.psum(dense_pre.astype(jnp.bfloat16), 'tp').astype(jnp.float32)  13.2 us
    all_gather x1, blocking collectives, local(): full_rows = lax.all_gather(arrived, 'tp', axis=2, tiled=True)  9.21 us
    all_to_all x1, waiting for transfers between devices, local(): lax.all_to_all(summed_out.reshape(arrived.shape), 'ep', split_axis=0, con...  7.21 us
    all_to_all x1, waiting for transfers between devices, local(): lax.all_to_all(outgoing, 'ep', split_axis=0, concat_axis=0, tiled=True)  6.31 us
  transfers between devices with their start and end apart: 6, of which 6 were waited for; matrix products, arithmetic and copies ran while one was open for 6% of the time, Pallas kernels for 0%

commit v1 on v0

--- a/solution.py
+++ b/solution.py
@@ -107,7 +107,13 @@
     mix_gate = jax.nn.sigmoid(scale_two * gate_dot)
     residual = settle(residual_f)
     normed = (residual_f * scale_two[:, None] * gain_rows[2]).astype(jnp.bfloat16)
-    rows_in = lax.all_gather(normed, "ep", axis=0, tiled=True)
+
+    def push_edge(w_in):
+        block_out = jnp.stack(tuple((w_in for _ in range(lax.psum(1, "ep")))), 0)
+        u1 = jnp.concatenate(lax.all_to_all(block_out, "ep", 0, 0), axis=0)
+        return u1
+
+    rows_in = push_edge(normed)
     dense_pre = jnp.concatenate(
         [
             jnp.dot(rows_in, dense_gate, preferred_element_type=jnp.float32),

time: 238 us -> 226 us (0.950)
  blocking collectives: 51.8 us -> 30.7 us
  waiting for transfers between devices: 121 us -> 132 us
    all_gather x1 -> x0, blocking collectives: 31.2 us -> none  [local(): rows_in = lax.all_gather(normed, 'ep', axis=0, tiled=True)]
    psum x1, waiting for transfers between devices: 13.2 us -> 29.9 us  [local(): lax.psum(dense_pre.astype(jnp.bfloat16), 'tp').astype(jnp.float32)]
    all_to_all x0 -> x1, blocking collectives: none -> 12.8 us  [local(): lax.all_to_all(outgoing, 'ep', split_axis=0, concat_axis=0, tiled=True)]
    all_to_all x1, waiting for transfers between devices: 6.31 us -> 0.01 us  [push_edge(): u1 = jnp.concatenate(lax.all_to_all(block_out, 'ep', 0, 0), axis=0)]
    all_gather x1, blocking collectives: 9.21 us -> 6.5 us  [local(): full_rows = lax.all_gather(arrived, 'tp', axis=2, tiled=True)]
  transfers between devices with their start and end apart: 6 -> 6, of which waited for: 6 -> 5; matrix products, arithmetic and copies ran while one was open for 6% -> 6% of each run, Pallas kernels for 0% -> 0%
where the time goes in v1:
time: 226 us; the launch traced here: 225 us
  waiting for transfers between devices  132 us (58%)
  blocking collectives  30.7 us (14%)
  matrix products  20.3 us (9%)
  between operations  14.1 us (6%)
  other arithmetic  13.3 us (6%)
  starting transfers between devices  9.09 us (4%)
  local copies, waits for them, and re-layouts  6.02 us (3%)
    reduce_scatter x1, waiting for transfers between devices, local(): lax.psum_scatter(jnp.dot(dense_hidden, dense_down, preferred_element_type...  52.6 us
    psum x1, waiting for transfers between devices, local(): lax.psum(dense_pre.astype(jnp.bfloat16), 'tp').astype(jnp.float32)  29.9 us
    reduce_scatter x1, waiting for transfers between devices, local(): lax.psum_scatter(partial_out.astype(jnp.bfloat16), 'tp', scatter_dimensio...  21.8 us
    reduce_scatter x1, waiting for transfers between devices, local(): lax.psum_scatter(branch_terms.astype(jnp.bfloat16), 'tp', scatter_dimensi...  20.2 us
    all_to_all x1, blocking collectives, local(): lax.all_to_all(outgoing, 'ep', split_axis=0, concat_axis=0, tiled=True)  12.8 us
    all_to_all x1, waiting for transfers between devices, local(): lax.all_to_all(summed_out.reshape(arrived.shape), 'ep', split_axis=0, con...  7.21 us
    all_gather x1, blocking collectives, local(): full_rows = lax.all_gather(arrived, 'tp', axis=2, tiled=True)  6.5 us
    psum x1, blocking collectives, local(): lax.psum((jnp.sum(branch * branch, axis=-1), jnp.sum(start_part * start_p...  5.77 us
  transfers between devices with their start and end apart: 6, of which 5 were waited for; matrix products, arithmetic and copies ran while one was open for 6% of the time, Pallas kernels for 0%

profile of v1, /device:TPU:0, one launch (start us, length us, event | category | flops | bytes accessed | tf_op | source)
XLA Modules:
  0.0 225.4 jit_solution(14164647654718429475)
XLA Ops:
  7.2 0.0 copy-start
  7.2 0.0 copy-start.2
  7.2 0.0 reduce-scatter.4.cloned.1.call-start
  7.3 0.9 slice.14
  8.2 1.0 multiply_reduce_fusion
  9.2 1.6 convolution_convert_fusion.7
  10.9 1.1 fusion.44
  12.0 0.7 dynamic_slice.21
  12.8 1.2 subtract_exponential_fusion
  13.9 0.0 copy-start.7
  14.0 0.1 copy.32
  14.0 0.1 copy.31
  14.1 1.6 convolution_convert_fusion.6
  15.8 1.6 convolution_convert_fusion.5
  17.5 0.8 fusion.38
  18.2 0.1 copy.42
  18.3 0.1 copy.34
  18.4 0.3 convolution_convert_fusion.8
  18.7 3.7 %multiply_add_fusion = f32[32,2,128,128]{3,2,1,0:T(8,128)S(1)} fusion(f32[32,2,128,128]{3,2,1,0:T(8,128)} %param.32, f32[32,2,128]{2,1,0:T(2,128)S(1)} %reshape.118, f32[32,2,128]{2,1,0:T(2,128)S(1)} %get-tuple-element.20, f32[32,2]{1,0:T(8,128)S(1)} %copy.31), kind=kLoop, calls=%fused_computation | loop fusion | flops 3145728 | bytes 8454400 | tf_op jit(solution)/shard_map/add | solution.py:72
  22.5 0.0 copy-start.1
  22.5 2.0 copy-done.1
  24.5 0.6 fusion.57
  25.1 0.1 broadcast_divide_fusion
  25.2 0.9 convolution_convert_fusion
  26.2 0.0 reduce-scatter.4.cloned.1.call-update
  26.2 0.1 copy.35
  26.3 0.1 reshape.109
  26.4 0.1 fusion.40
  26.5 0.1 reduce_window_sum.11
  26.6 0.2 select_reduce_fusion
  26.8 0.9 fusion.56
  27.7 0.8 dynamic-slice_multiply_fusion
  28.5 20.2 %reduce-scatter.4.cloned.1.call-done = bf16[32,512]{1,0:T(8,128)(2,1)} async-done(((bf16[32,2048]{1,0:T(8,128)(2,1)}), bf16[32,512]{1,0:T(8,128)(2,1)}) %reduce-scatter.4.cloned.1.call-update) | async-done | bytes 32784 | tf_op jit(solution)/shard_map/reduce_scatter | solution.py:83
  48.7 1.0 multiply_reduce_fusion.2
  49.7 5.8 %all-reduce = (f32[32]{0:T(128)S(1)}, f32[32]{0:T(128)S(1)}, f32[32]{0:T(128)S(1)}, f32[32]{0:T(128)S(1)}, f32[32]{0:T(128)S(1)}, /*index=5*/f32[32]{0:T(128)S(1)}) all-reduce(f32[32]{0:T(128)S(1)} %get-tuple-element.9, f32[32]{0:T(128)S(1)} %get-tuple-element.8, f32[32]{0:T(128)S(1)} %get-tuple-element.5, ...), channel_id=1, replica_groups=mesh['ep'=8,'tp'=4] {'tp'}, use_global_device_ids=true, to_apply=%region_3.4 | all-reduce | flops 192 | bytes 1536 | tf_op jit(solution)/shard_map/psum | solution.py:91
  55.5 0.9 multiply_convert_fusion.1
  56.4 0.2 convolution_convert_fusion.4
  56.6 12.8 %all_to_all.15 = bf16[8,16,512]{2,1,0:T(8,128)(2,1)S(1)} all-to-all(bf16[8,16,512]{2,1,0:T(8,128)(2,1)S(1)} %bitcast.57), channel_id=1, replica_groups=mesh['ep'=8,'tp'=4] {'ep'}, dimensions={0} | all-to-all | bytes 262144 | tf_op jit(solution)/shard_map/all_to_all | solution.py:151
  69.4 0.7 stack.2
  70.1 3.4 %all-to-all-start.2 = ((bf16[8,32,512]{2,1,0:T(8,128)(2,1)}), bf16[8,32,512]{2,1,0:T(8,128)(2,1)S(1)}, u32[]{:S(2)}, u32[]{:S(2)}) async-start(bf16[8,32,512]{2,1,0:T(8,128)(2,1)} %stack.2), calls=%async_computation.4 | async-start | bytes 524288 | tf_op jit(solution)/shard_map/all_to_all | solution.py:113
  73.5 0.0 all-reduce.3.cloned.1.call-start
  73.6 6.5 %all_gather.3 = bf16[8,16,2048]{2,1,0:T(8,128)(2,1)S(1)} all-gather(bf16[8,16,512]{2,1,0:T(8,128)(2,1)S(1)} %all_to_all.15), channel_id=1, replica_groups=mesh['ep'=8,'tp'=4] {'tp'}, dimensions={2}, use_global_device_ids=true | all-gather | bytes 655360 | tf_op jit(solution)/shard_map/all_gather | solution.py:152
  80.1 3.6 %fusion.4 = f32[128,896]{1,0:T(8,128)} fusion(bf16[128,2048]{1,0:T(8,128)(2,1)S(1)} %bitcast.54, bf16[1,2048,896]{2,1,0:T(8,128)(2,1)} %param.37), kind=kOutput, calls=%fused_computation.5 | convolution fusion | flops 469762048 | bytes 4653056 | tf_op jit(solution)/shard_map/dot_general | solution.py:154
  83.6 0.4 convolution_convert_fusion.1
  84.0 0.4 convolution_convert_fusion.2
  84.4 0.9 pad_maximum_fusion
  85.3 0.0 all-reduce.3.cloned.1.call-update
  85.4 0.0 reduce-scatter.6.cloned.1.call-start
  85.4 5.5 %fusion.6 = bf16[128,2048]{1,0:T(8,128)(2,1)} fusion(bf16[1,896,2048]{2,1,0:T(8,128)(2,1)} %param.39, bf16[128,2048]{1,0:T(8,128)(2,1)S(1)} %bitcast.55, bf16[1,2048,896]{2,1,0:T(8,128)(2,1)} %param.38, f32[128,896]{1,0:T(8,128)} %fusion.4), kind=kOutput, calls=%fused_computation.7 | convolution fusion | flops 940474368 | bytes 8847360 | tf_op jit(solution)/shard_map/dot_general | solution.py:157
  90.9 0.0 reduce-scatter.6.cloned.1.call-update
  90.9 0.0 reduce-scatter.8.cloned.1.call-start
  91.0 29.9 %all-reduce.3.cloned.1.call-done = bf16[256,1408]{0,1:T(8,128)(2,1)} async-done(((bf16[256,1408]{0,1:T(8,128)(2,1)}), bf16[256,1408]{0,1:T(8,128)(2,1)}) %all-reduce.3.cloned.1.call-update) | async-done | bytes 720912 | tf_op jit(solution)/shard_map/psum | solution.py:124
  120.9 1.2 convert_element_type.94
  122.2 1.1 convolution_convert_fusion.3
  123.3 0.0 reduce-scatter.8.cloned.1.call-update
  123.3 21.8 %reduce-scatter.6.cloned.1.call-done = bf16[128,512]{1,0:T(8,128)(2,1)} async-done(((bf16[128,2048]{1,0:T(8,128)(2,1)}), bf16[128,512]{1,0:T(8,128)(2,1)}) %reduce-scatter.6.cloned.1.call-update) | async-done | bytes 131088 | tf_op jit(solution)/shard_map/reduce_scatter | solution.py:158
  145.1 5.5 %all-to-all-start.1 = ((bf16[8,16,512]{2,1,0:T(8,128)(2,1)}), bf16[8,16,512]{2,1,0:T(8,128)(2,1)S(1)}, u32[]{:S(2)}, u32[]{:S(2)}) async-start(bf16[8,16,512]{2,1,0:T(8,128)(2,1)} %bitcast.66), calls=%async_computation.3 | async-start | bytes 262144 | tf_op jit(solution)/shard_map/all_to_all | solution.py:161
  150.6 0.1 iota_compare_fusion.3
  150.8 7.2 %all-to-all-done.1 = bf16[8,16,512]{2,1,0:T(8,128)(2,1)S(1)} async-done(((bf16[8,16,512]{2,1,0:T(8,128)(2,1)}), bf16[8,16,512]{2,1,0:T(8,128)(2,1)S(1)}, u32[]{:S(2)}, u32[]{:S(2)}) %all-to-all-start.1) | async-done | bytes 131104 | tf_op jit(solution)/shard_map/all_to_all | solution.py:161
  158.0 0.2 fusion.15
  158.1 52.6 %reduce-scatter.8.cloned.1.call-done = bf16[32,512]{1,0:T(8,128)(2,1)} async-done(((bf16[256,512]{1,0:T(8,128)(2,1)}), bf16[32,512]{1,0:T(8,128)(2,1)}) %reduce-scatter.8.cloned.1.call-update) | async-done | bytes 32784 | tf_op jit(solution)/shard_map/reduce_scatter | solution.py:127
  210.8 0.9 multiply_reduce_fusion.1
  211.7 5.7 %psum.63 = f32[32]{0:T(128)S(1)} all-reduce(f32[32]{0:T(128)S(1)} %multiply_reduce_fusion.1), channel_id=1, replica_groups=mesh['ep'=8,'tp'=4] {'tp'}, use_global_device_ids=true, to_apply=%region_22.23 | all-reduce | flops 32 | bytes 256 | tf_op jit(solution)/shard_map/psum | solution.py:175
  217.4 1.5 add_convert_fusion
  (34 shorter events, 0.3 us)
Async XLA Ops:
  7.2 18.1 %copy-start = (bf16[256,2048]{1,0:T(8,128)(2,1)S(1)}, bf16[256,2048]{1,0:T(8,128)(2,1)}, u32[]{:S(2)}) copy-start(bf16[256,2048]{1,0:T(8,128)(2,1)} %param.31) | copy-start | bytes 3145732
  7.2 11.2 %copy-start.2 = (bf16[32,2048]{1,0:T(8,128)(2,1)S(1)}, bf16[32,2048]{1,0:T(8,128)(2,1)}, u32[]{:S(2)}) copy-start(bf16[32,2048]{1,0:T(8,128)(2,1)} %param.22) | copy-start | bytes 393220
  7.2 10.3 %copy-start.6 = (f32[32,2,128]{2,1,0:T(2,128)S(1)}, f32[32,2,128]{2,1,0:T(2,128)}, u32[]{:S(2)}) copy-start(f32[32,2,128]{2,1,0:T(2,128)} %param.33) | copy-start | bytes 98308
  7.2 11.2 %copy-start.3 = (bf16[2048,256]{1,0:T(8,128)(2,1)S(1)}, bf16[2048,256]{1,0:T(8,128)(2,1)}, u32[]{:S(2)}) copy-start(bf16[2048,256]{1,0:T(8,128)(2,1)} %param.27) | copy-start | bytes 3145732
  7.2 41.5 %reduce-scatter.4.cloned.1.call-start = ((), (), s32[]{:S(2)}) async-start(), calls=%async_computation.6 | async-start | bytes 163840 | tf_op jit(solution)/shard_map/reduce_scatter | solution.py:83
  13.9 8.5 %copy-start.7 = (f32[32,2]{0,1:T(2,128)}, f32[32,2]{0,1:T(2,128)S(1)}, u32[]{:S(2)}) copy-start(f32[32,2]{0,1:T(2,128)S(1)} %get-tuple-element.22) | copy-start | bytes 772
  22.5 2.0 copy-start.1
  24.5 1.7 copy-start.9
  27.7 56.0 %copy-start.4 = (bf16[512,704]{0,1:T(8,128)(2,1)S(1)}, bf16[512,704]{0,1:T(8,128)(2,1)}, u32[]{:S(2)}) copy-start(bf16[512,704]{0,1:T(8,128)(2,1)} %param.41) | copy-start | bytes 2162692
  69.4 14.6 %copy-start.5 = (bf16[512,704]{0,1:T(8,128)(2,1)S(1)}, bf16[512,704]{0,1:T(8,128)(2,1)}, u32[]{:S(2)}) copy-start(bf16[512,704]{0,1:T(8,128)(2,1)} %param.40) | copy-start | bytes 2162692
  70.1 13.5 %all-to-all-start.2 = ((bf16[8,32,512]{2,1,0:T(8,128)(2,1)}), bf16[8,32,512]{2,1,0:T(8,128)(2,1)S(1)}, u32[]{:S(2)}, u32[]{:S(2)}) async-start(bf16[8,32,512]{2,1,0:T(8,128)(2,1)} %stack.2), calls=%async_computation.4 | async-start | bytes 524288 | tf_op jit(solution)/shard_map/all_to_all | solution.py:113
  73.5 47.4 %all-reduce.3.cloned.1.call-start = ((), (), s32[]{:S(2)}) async-start(), calls=%async_computation.8 | async-start | bytes 1441792 | tf_op jit(solution)/shard_map/psum | solution.py:124
  85.4 36.8 %copy-start.10 = (bf16[704,512]{1,0:T(8,128)(2,1)S(1)}, bf16[704,512]{1,0:T(8,128)(2,1)}, u32[]{:S(2)}) copy-start(bf16[704,512]{1,0:T(8,128)(2,1)} %param.42) | copy-start | bytes 2162692
  85.4 59.7 %reduce-scatter.6.cloned.1.call-start = ((), (), s32[]{:S(2)}) async-start(), calls=%async_computation.7 | async-start | bytes 655360 | tf_op jit(solution)/shard_map/reduce_scatter | solution.py:158
  90.9 59.8 %copy-start.8 = (f32[32,2]{0,1:T(2,128)S(1)}, f32[32,2]{0,1:T(2,128)}, u32[]{:S(2)}) copy-start(f32[32,2]{0,1:T(2,128)} %param.36) | copy-start | bytes 772
  90.9 119.8 %reduce-scatter.8.cloned.1.call-start = ((), (), s32[]{:S(2)}) async-start(), calls=%async_computation.9 | async-start | bytes 294912 | tf_op jit(solution)/shard_map/reduce_scatter | solution.py:127
  145.1 12.9 %all-to-all-start.1 = ((bf16[8,16,512]{2,1,0:T(8,128)(2,1)}), bf16[8,16,512]{2,1,0:T(8,128)(2,1)S(1)}, u32[]{:S(2)}, u32[]{:S(2)}) async-start(bf16[8,16,512]{2,1,0:T(8,128)(2,1)} %bitcast.66), calls=%async_computation.3 | async-start | bytes 262144 | tf_op jit(solution)/shard_map/all_to_all | solution.py:161
Sparse Core Ops, SparseCore 0:
  26.3 22.3 reduce-scatter.3
  85.5 35.3 all-reduce.2
  123.4 21.6 reduce-scatter.5
  148.3 62.4 reduce-scatter.7
